TPU v7x, 32 devices: a whole 2x2x4 slice. The times are simulated.
32 devices in a mesh: grp: 2 (over y), ep: 4 (over z), tp: 4 (over x, core).
Axes of the slice: x: 2, y: 2, z: 4, core: 2. Of those that a mesh axis runs over, the one named last changes fastest.
Arguments:
- tokens: bfloat16 [80, 1024], P(('grp', 'ep')), parts along dimension 0, may hold values from -40 to 40
- attn_gain: float32 [1024], replicated, may hold values from 0.1 to 1.9
- w_query: bfloat16 [1024, 1024], P(None, 'tp'), may hold values from -0.1875 to 0.1875
- w_key: bfloat16 [1024, 512], P(None, 'tp'), may hold values from -0.1875 to 0.1875
- w_value: bfloat16 [1024, 512], P(None, 'tp'), may hold values from -0.1875 to 0.1875
- key_cache: bfloat16 [80, 512, 1024], P(('grp', 'ep'), 'tp'), parts along dimension 0, may hold values from -6 to 6
- value_cache: bfloat16 [80, 512, 1024], P(('grp', 'ep'), 'tp'), parts along dimension 0, may hold values from -6 to 6
- lengths: int32 [80], P(('grp', 'ep')), parts along dimension 0, may hold values from 256 to 1024
- head_bias: float32 [16], P('tp'), may hold values from -8 to -2
- w_out: bfloat16 [1024, 1024], P(None, 'tp'), may hold values from -0.1875 to 0.1875
- ffn_gain: float32 [1024], replicated, may hold values from 0.1 to 1.9
- route_ids: int32 [80, 2], P(('grp', 'ep')), parts along dimension 0, may hold values from 0 to 3, all different within a row; in each aligned block of 10 rows (0 to 9, 10 to 19, ...) at most 10 rows name the same one
- route_weights: float32 [80, 2], P(('grp', 'ep')), parts along dimension 0, may hold values from 0.1 to 1
- w_gate: bfloat16 [4, 1024, 2048], P('ep', None, 'tp'), may hold values from -0.1875 to 0.1875
- w_up: bfloat16 [4, 1024, 2048], P('ep', None, 'tp'), may hold values from -0.1875 to 0.1875
- w_down: bfloat16 [4, 2048, 1024], P('ep', 'tp'), may hold values from -0.125 to 0.125
Outputs:
- mixed: bfloat16 [80, 1024], P(('grp', 'ep'), 'tp'), parts along dimension 0
- new_keys: bfloat16 [80, 512], P(('grp', 'ep'), 'tp'), parts along dimension 0
- new_values: bfloat16 [80, 512], P(('grp', 'ep'), 'tp'), parts along dimension 0
There are 2 independent parts, one for each index of `grp`. A program takes and returns all parts, laid end to end along the dimension named above; an argument that names none is the same for every part. Nothing has to cross between parts.
Inputs may be any that keep to these rules, and one draw needn't show every extreme that they name: `route_ids`: each row names 2 different experts. In each aligned block of 10 rows no expert is named more than 10 times, and in some block some expert is named exactly 10 times.
All inputs are finite; a program needn't handle non-finite values.
Results may differ from a plain program's by a relative error of at most 0.012.
Values may be sent and summed in bfloat16 or wider, within the bound.
A program may use at most 64 MiB of HBM per device.

v0:
```python
import functools

import jax
import jax.numpy as jnp
from jax import lax
from jax.experimental import pallas as pl
from jax.experimental.pallas import tpu as pltpu
from jax.sharding import PartitionSpec as P

HEAD_SIZE = 64
EPSILON = 1e-06
ROW_TILE = 16
MESH_IDS = pl.DeviceIdType.MESH
F32 = jnp.float32
BF16 = jnp.bfloat16


def iota(shape, dim):
    return lax.broadcasted_iota(jnp.int32, shape, dim)


def dot(a, b):
    return jnp.dot(a, b, preferred_element_type=F32)


def layer_kernel(
    n_ep,
    n_tp,
    tokens_hbm,
    attn_gain_hbm,
    w_query_hbm,
    w_key_hbm,
    w_value_hbm,
    key_hbm,
    value_hbm,
    lengths_hbm,
    head_bias_hbm,
    w_out_hbm,
    ffn_gain_hbm,
    route_ids_hbm,
    route_weights_hbm,
    w_gate_hbm,
    w_up_hbm,
    w_down_hbm,
    mixed_ref,
    new_keys_ref,
    new_values_ref,
    tokens,
    attn_gain,
    w_query,
    w_key,
    w_value,
    keys,
    values,
    lengths,
    head_bias,
    w_out,
    ffn_gain,
    route_ids,
    route_weights,
    w_gate,
    w_up,
    w_down,
    token_rows,
    head_part,
    head_all,
    hidden_part,
    hidden_all,
    ffn_rows,
    out_parts,
    returned,
    small_sem,
    pair_sem,
    weight_sem,
    send_sem,
    recv_sem,
):
    ep = lax.axis_index("ep")
    tp = lax.axis_index("tp")
    me = ep * n_tp + tp
    n_peers = n_ep * n_tp
    rows = tokens.shape[0]
    query_cols = w_query.shape[1]
    key_cols = w_key.shape[1]
    heads = query_cols // HEAD_SIZE
    group = query_cols // key_cols
    slice_width = w_out.shape[1]
    cache_len = keys.shape[2]
    pairs = rows // 2

    def far_ep(step):
        from_top = jnp.where(n_ep - 1 - step > ep, n_ep - 1 - step, n_ep - 2 - step)
        from_bottom = jnp.where(step < ep, step, step + 1)
        return jnp.where(2 * ep < n_ep, from_top, from_bottom)

    def other_tp(step):
        chip = lax.rem(tp // 2 + 1 + step // 2, n_tp // 2)
        return chip * 2 + lax.rem(tp + step, 2)

    tp_order = [other_tp(step) for step in range(n_tp - 2)]
    tp_order += [other_tp(n_tp - 1), tp]

    def each_peer(fn):
        def to_ep(step):
            for peer_tp in tp_order:
                fn(far_ep(step), peer_tp)

        if n_peers <= 16:
            for step in range(n_ep - 1):
                to_ep(step)
        else:
            pl.loop(0, n_ep - 1)(to_ep)
        for peer_tp in tp_order[:-1]:
            fn(ep, peer_tp)

    barrier = pltpu.get_barrier_semaphore()

    def greet(peer_ep, peer_tp):
        pl.semaphore_signal(
            barrier,
            inc=1,
            device_id={"ep": peer_ep, "tp": peer_tp},
            device_id_type=MESH_IDS,
        )

    ffn_rows[...] = jnp.zeros_like(ffn_rows)
    each_peer(greet)

    small = []
    for number, (source, target) in enumerate(
        (
            (tokens_hbm, tokens),
            (attn_gain_hbm, attn_gain),
            (w_query_hbm, w_query),
            (w_key_hbm, w_key),
            (w_value_hbm, w_value),
            (lengths_hbm, lengths),
            (head_bias_hbm, head_bias),
            (ffn_gain_hbm, ffn_gain),
            (route_ids_hbm, route_ids),
            (route_weights_hbm, route_weights),
        )
    ):
        copy = pltpu.make_async_copy(source, target, small_sem.at[number])
        if number not in (3, 4):
            copy.start()
        small.append(copy)
    key_copies, value_copies, weight_copies = [], [], []
    for pair in range(pairs):
        part = pl.ds(2 * pair, 2)
        copy = pltpu.make_async_copy(key_hbm.at[part], keys.at[part], pair_sem.at[pair])
        copy.start()
        key_copies.append(copy)
    for pair in range(pairs):
        part = pl.ds(2 * pair, 2)
        copy = pltpu.make_async_copy(
            value_hbm.at[part], values.at[part], pair_sem.at[pairs + pair]
        )
        copy.start()
        value_copies.append(copy)
    small[3].start()
    small[4].start()
    for number, (source, target) in enumerate(
        (
            (w_out_hbm, w_out),
            (w_gate_hbm, w_gate),
            (w_up_hbm, w_up),
            (w_down_hbm, w_down),
        )
    ):
        copy = pltpu.make_async_copy(source, target, weight_sem.at[number])
        copy.start()
        weight_copies.append(copy)

    block_len = 256 if cache_len % 256 == 0 else 128
    n_blocks = cache_len // block_len
    triangle = (
        iota((block_len, block_len), 0) > iota((block_len, block_len), 1)
    ).astype(BF16)
    flat = rows * heads
    expand = (iota((flat, ROW_TILE), 0) // heads == iota((flat, ROW_TILE), 1)).astype(BF16)
    collapse = (iota((ROW_TILE, flat), 1) // heads == iota((ROW_TILE, flat), 0)).astype(BF16)
    own_head = iota((flat, query_cols), 1) // HEAD_SIZE == lax.rem(
        iota((flat, query_cols), 0), heads
    )
    fold_row = iota((query_cols, key_cols), 0)
    fold_col = iota((query_cols, key_cols), 1)
    fold = (
        (fold_row // (HEAD_SIZE * group)) * HEAD_SIZE + lax.rem(fold_row, HEAD_SIZE)
        == fold_col
    ).astype(BF16)
    unfold_row = iota((key_cols, query_cols), 0)
    unfold_col = iota((key_cols, query_cols), 1)
    unfold = (
        (unfold_col // (HEAD_SIZE * group)) * HEAD_SIZE + lax.rem(unfold_col, HEAD_SIZE)
        == unfold_row
    ).astype(BF16)
    odd = lax.rem(iota((flat, key_cols), 0) // heads, 2) == 1

    small[0].wait()
    token_rows[...] = jnp.zeros_like(token_rows)
    token_rows[:rows, :] = tokens[...].astype(F32)
    rows_f32 = token_rows[...]
    small[1].wait()
    normed = (
        rows_f32
        * lax.rsqrt(jnp.mean(rows_f32 * rows_f32, axis=1, keepdims=True) + EPSILON)
        * attn_gain[...]
    ).astype(BF16)
    small[2].wait()
    queries = dot(normed, w_query[...]).astype(BF16)
    spread = jnp.where(own_head, dot(expand, queries), 0.0).astype(BF16)
    folded = dot(spread, fold)
    left = jnp.where(odd, 0.0, folded).astype(BF16)
    right = jnp.where(odd, folded, 0.0).astype(BF16)

    small[5].wait()
    small[6].wait()
    row_col = iota((flat, 1), 0)
    length_col = jnp.zeros((flat, 1), jnp.int32)
    for row in range(rows):
        length_col = jnp.where(row_col // heads == row, lengths[row], length_col)
    bias_col = jnp.zeros((flat, 1), F32)
    for head in range(heads):
        bias_col = jnp.where(lax.rem(row_col, heads) == head, head_bias[head], bias_col)
    pieces = []
    for pair in range(pairs):
        key_copies[pair].wait()
        part = slice(2 * heads * pair, 2 * heads * (pair + 1))
        block = keys[2 * pair : 2 * pair + 2].reshape(2 * key_cols, cache_len)
        query_block = jnp.concatenate([left[part], right[part]], axis=1)
        pieces.append(dot(query_block, block))
    scores = jnp.concatenate(pieces, axis=0) * HEAD_SIZE ** (-0.5) + bias_col

    in_cache = iota((flat, cache_len), 1) < length_col
    soft = jnp.log(1.0 + jnp.exp(-jnp.abs(scores)))
    log_rest = jnp.where(in_cache, jnp.minimum(-scores, 0.0) - soft, 0.0)
    log_take = jnp.minimum(scores, 0.0) - soft
    high = log_rest.astype(BF16)
    low = (log_rest - high.astype(F32)).astype(BF16)
    stacked = jnp.concatenate(
        [
            part[:, block * block_len : (block + 1) * block_len]
            for part in (high, low)
            for block in range(n_blocks)
        ],
        axis=0,
    )
    within = dot(stacked, triangle)
    carried = jnp.zeros((flat, 1), F32)
    tails = [None] * n_blocks
    for block in reversed(range(n_blocks)):
        inner = (
            within[block * flat : (block + 1) * flat]
            + within[(n_blocks + block) * flat : (n_blocks + block + 1) * flat]
        )
        tails[block] = inner + carried
        first = block * block_len
        carried = carried + inner[:, :1] + log_rest[:, first : first + 1]
    tail_sum = jnp.concatenate(tails, axis=1)
    breaks = jnp.where(in_cache, jnp.exp(log_take + tail_sum), 0.0).astype(BF16)

    for copy in value_copies:
        copy.wait()
    value_rows = values[...].reshape(rows * key_cols, cache_len)
    crossed = dot(value_rows, breaks.T).T
    own = jnp.zeros((flat, key_cols), F32)
    for row in range(rows):
        part = slice(row * key_cols, (row + 1) * key_cols)
        own = jnp.where(row_col // heads == row, crossed[:, part], own)
    own = own.astype(BF16)
    unfolded = jnp.where(own_head, dot(own, unfold), 0.0).astype(BF16)
    heads_out = dot(collapse, unfolded).astype(BF16)

    pl.semaphore_wait(barrier, n_peers - 1)
    head_part[...] = heads_out[:rows]
    own_cols = pl.ds(pl.multiple_of(tp * query_cols, query_cols), query_cols)
    head_slot = head_all.at[:, own_cols]
    for peer_tp in tp_order[:-1]:
        pltpu.make_async_remote_copy(
            src_ref=head_part,
            dst_ref=head_slot,
            send_sem=send_sem.at[0],
            recv_sem=recv_sem.at[0],
            device_id={"tp": peer_tp},
            device_id_type=MESH_IDS,
        ).start()
    pltpu.make_async_copy(head_part, head_slot, recv_sem.at[0]).start()
    small[3].wait()
    small[4].wait()
    new_keys_ref[...] = dot(normed, w_key[...]).astype(BF16)[:rows]
    new_values_ref[...] = dot(normed, w_value[...]).astype(BF16)[:rows]
    weight_copies[0].wait()
    pltpu.make_async_copy(head_all, head_all, recv_sem.at[0]).wait()
    attn_out = dot(head_all[...], w_out[...])

    slice_cols = pl.ds(pl.multiple_of(tp * slice_width, slice_width), slice_width)
    own_hidden = token_rows[:rows, slice_cols] + attn_out
    hidden_part[...] = own_hidden.astype(BF16)
    hidden_slot = hidden_all.at[ep, :, slice_cols]

    def send_hidden(peer_ep, peer_tp):
        pltpu.make_async_remote_copy(
            src_ref=hidden_part,
            dst_ref=hidden_slot,
            send_sem=send_sem.at[1],
            recv_sem=recv_sem.at[1],
            device_id={"ep": peer_ep, "tp": peer_tp},
            device_id_type=MESH_IDS,
        ).start()

    each_peer(send_hidden)
    pltpu.make_async_copy(hidden_part, hidden_slot, recv_sem.at[1]).start()
    for copy in small[7:]:
        copy.wait()
    diagonal = iota((rows, rows), 0) == iota((rows, rows), 1)
    choices = []
    for choice in range(route_ids.shape[0]):
        id_row = route_ids[choice : choice + 1, :].astype(F32)
        weight_row = route_weights[choice : choice + 1, :]
        choices.append(
            tuple(
                jnp.sum(jnp.where(diagonal, row, 0.0), axis=1, keepdims=True)
                for row in (id_row, weight_row)
            )
        )
    for copy in weight_copies[1:]:
        copy.wait()
    pltpu.make_async_copy(hidden_all, hidden_all, recv_sem.at[1]).wait()
    for source in range(n_ep):
        hidden = hidden_all[source].astype(F32)
        first = source * ROW_TILE
        ffn_rows[first : first + rows, :] = (
            hidden
            * lax.rsqrt(jnp.mean(hidden * hidden, axis=1, keepdims=True) + EPSILON)
            * ffn_gain[...]
        ).astype(BF16)
    ffn_in = ffn_rows[...]

    gate_act = dot(ffn_in, w_gate[0])
    up_act = dot(ffn_in, w_up[0])
    hidden_act = (gate_act / (1.0 + jnp.exp(-gate_act)) * up_act).astype(BF16)
    for step in range(n_tp):
        to_tp = tp_order[step]
        part = pl.ds(pl.multiple_of(to_tp * slice_width, slice_width), slice_width)
        partial_out = dot(hidden_act, w_down[0, :, part]).astype(BF16)
        for owner in range(n_ep):
            first = owner * ROW_TILE
            out_parts[step, owner] = partial_out[first : first + rows]

        def send_out(to_ep):
            pltpu.make_async_remote_copy(
                src_ref=out_parts.at[step, to_ep],
                dst_ref=returned.at[me],
                send_sem=send_sem.at[2],
                recv_sem=recv_sem.at[2],
                device_id={"ep": to_ep, "tp": to_tp},
                device_id_type=MESH_IDS,
            ).start()

        if n_ep <= 8:
            for hop in range(n_ep - 1):
                send_out(far_ep(hop))
        else:

            @pl.loop(0, n_ep - 1)
            def _(hop):
                send_out(far_ep(hop))

        if step < n_tp - 1:
            send_out(ep)
        else:
            pltpu.make_async_copy(
                out_parts.at[step, ep],
                returned.at[me],
                recv_sem.at[2],
            ).start()
    pltpu.make_async_copy(returned, returned, recv_sem.at[2]).wait()
    mixed = own_hidden
    for expert in range(n_ep):
        total = returned[expert * n_tp].astype(F32)
        for number in range(1, n_tp):
            total = total + returned[expert * n_tp + number].astype(F32)
        scale = jnp.zeros((rows, 1), F32)
        for id_col, weight_col in choices:
            scale = scale + jnp.where(id_col == expert, weight_col, 0.0)
        mixed = mixed + scale * total.astype(BF16).astype(F32)
    mixed_ref[...] = mixed.astype(BF16)

    sent = head_all.at[:, pl.ds(0, (n_tp - 1) * query_cols)]
    pltpu.make_async_copy(sent, sent, send_sem.at[0]).wait()
    sent = returned.at[pl.ds(0, n_peers - 1)]
    pltpu.make_async_copy(sent, sent, send_sem.at[1]).wait()
    pltpu.make_async_copy(sent, sent, send_sem.at[2]).wait()


def place_results(*refs):
    copies = [
        pltpu.make_async_copy(refs[number], refs[3 + number], refs[6].at[number])
        for number in range(3)
    ]
    for copy in copies:
        copy.start()
    for copy in copies:
        copy.wait()


def shards(
    tokens,
    attn_gain,
    w_query,
    w_key,
    w_value,
    key_cache,
    value_cache,
    lengths,
    head_bias,
    w_out,
    ffn_gain,
    route_ids,
    route_weights,
    w_gate,
    w_up,
    w_down,
):
    n_ep = lax.axis_size("ep")
    n_tp = lax.axis_size("tp")
    rows, width = tokens.shape
    query_cols = w_query.shape[1]
    key_cols = w_key.shape[1]
    slice_width = w_out.shape[1]
    operands = (
        tokens,
        attn_gain.reshape(1, width),
        w_query,
        w_key,
        w_value,
        key_cache,
        value_cache,
        lengths,
        head_bias,
        w_out,
        ffn_gain.reshape(1, width),
        route_ids.T,
        route_weights.T,
        w_gate,
        w_up,
        w_down,
    )
    in_smem = (7, 8)
    buffers = [
        (pltpu.SMEM if number in in_smem else pltpu.VMEM)(operand.shape, operand.dtype)
        for number, operand in enumerate(operands)
    ]
    n_peers = n_ep * n_tp
    scratch = buffers + [
        pltpu.VMEM((ROW_TILE, width), F32),
        pltpu.VMEM((rows, query_cols), BF16),
        pltpu.VMEM((rows, query_cols * n_tp), BF16),
        pltpu.VMEM((rows, slice_width), BF16),
        pltpu.VMEM((n_ep, rows, width), BF16),
        pltpu.VMEM((n_ep * ROW_TILE, width), BF16),
        pltpu.VMEM((n_tp, n_ep, rows, slice_width), BF16),
        pltpu.VMEM((n_peers, rows, slice_width), BF16),
        pltpu.SemaphoreType.DMA((10,)),
        pltpu.SemaphoreType.DMA((rows,)),
        pltpu.SemaphoreType.DMA((4,)),
        pltpu.SemaphoreType.DMA((3,)),
        pltpu.SemaphoreType.DMA((3,)),
    ]
    results = pl.pallas_call(
        functools.partial(layer_kernel, n_ep, n_tp),
        out_shape=(
            pltpu.VMEM((rows, slice_width), BF16),
            pltpu.VMEM((rows, key_cols), BF16),
            pltpu.VMEM((rows, key_cols), BF16),
        ),
        in_specs=[pl.BlockSpec(memory_space=pltpu.HBM)] * len(operands),
        out_specs=tuple([pl.BlockSpec(memory_space=pltpu.VMEM)] * 3),
        scratch_shapes=scratch,
        compiler_params=pltpu.CompilerParams(
            collective_id=0, has_side_effects=True, vmem_limit_bytes=66990080
        ),
        name="layer",
    )(*operands)
    return pl.pallas_call(
        place_results,
        out_shape=tuple(jax.ShapeDtypeStruct(r.shape, r.dtype) for r in results),
        in_specs=[pl.BlockSpec(memory_space=pltpu.VMEM)] * 3,
        out_specs=tuple([pl.BlockSpec(memory_space=pltpu.HBM)] * 3),
        scratch_shapes=[pltpu.SemaphoreType.DMA((3,))],
        compiler_params=pltpu.CompilerParams(vmem_limit_bytes=2**20),
        name="place",
    )(*results)


def solution(mesh):
    in_specs = (
        P(("grp", "ep"), None),
        P(),
        P(None, "tp"),
        P(None, "tp"),
        P(None, "tp"),
        P(("grp", "ep"), "tp", None),
        P(("grp", "ep"), "tp", None),
        P(("grp", "ep")),
        P("tp"),
        P(None, "tp"),
        P(),
        P(("grp", "ep"), None),
        P(("grp", "ep"), None),
        P("ep", None, "tp"),
        P("ep", None, "tp"),
        P("ep", "tp", None),
    )
    out_specs = (P(("grp", "ep"), "tp"), P(("grp", "ep"), "tp"), P(("grp", "ep"), "tp"))
    return jax.shard_map(shards, mesh=mesh, in_specs=in_specs, out_specs=out_specs, check_vma=False)
```

profile of v0, /device:TPU:0, one launch (start us, length us, event | category | flops | bytes accessed | tf_op | source)
XLA Modules:
  0.0 22.9 jit_solution(8629524394111533425)
XLA Ops:
  0.6 21.6 %layer.1 = (bf16[10,256]{1,0:T(8,128)(2,1)S(1)}, bf16[10,128]{1,0:T(8,128)(2,1)S(1)}, bf16[10,128]{1,0:T(8,128)(2,1)S(1)}) custom-call(bf16[10,1024]{1,0:T(8,128)(2,1)} %tokens_hbm.1, f32[1,1024]{1,0:T(1,128)} %bitcast.4, bf16[1024,256]{1,0:T(8,128)(2,1)} %w_query_hbm.1, bf16[1024,128]{1,0:T(8,128)(2,1)} %w_key_hbm.1, bf16[1024,128]{1,0:T(8,128)(2,1)} %w_value_hbm.1, ...), custom_call_target="tpu_custom_call" | custom-call | tf_op jit(solution)/shard_map/layer/pallas_call | solution.py:471
  22.3 0.6 %place.1 = (bf16[10,256]{1,0:T(8,128)(2,1)}, bf16[10,128]{1,0:T(8,128)(2,1)}, bf16[10,128]{1,0:T(8,128)(2,1)}) custom-call(bf16[10,256]{1,0:T(8,128)(2,1)S(1)} %get-tuple-element.6.refs_0_, bf16[10,128]{1,0:T(8,128)(2,1)S(1)} %get-tuple-element.7.refs_1_, bf16[10,128]{1,0:T(8,128)(2,1)S(1)} %get-tuple-element.8.refs_2_), custom_call_target="tpu_custom_call" | custom-call | tf_op jit(solution)/shard_map/place/pallas_call | solution.py:486
where the time goes:
time: 23.1 us; the launch traced here: 22.9 us
  Pallas kernels  22.3 us (97%)
  between operations  0.65 us (3%)
    pallas_call x1, Pallas kernels, shards(): pl.pallas_call(functools.partial(layer_kernel, n_ep, n_tp), out_shape=(pl...  21.6 us
    pallas_call x1, Pallas kernels, shards(): pl.pallas_call(place_results, out_shape=tuple((jax.ShapeDtypeStruct(r.sha...  0.63 us

commit v1 on v0

--- a/solution.py
+++ b/solution.py
@@ -61,7 +61,7 @@
     w_gate,
     w_up,
     w_down,
-    token_rows,
+    spread,
     head_part,
     head_all,
     hidden_part,
@@ -81,7 +81,7 @@
     n_peers = n_ep * n_tp
     rows = tokens.shape[0]
     query_cols = w_query.shape[1]
-    key_cols = w_key.shape[1]
+    key_cols = w_key_hbm.shape[1]
     heads = query_cols // HEAD_SIZE
     group = query_cols // key_cols
     slice_width = w_out.shape[1]
@@ -123,54 +123,52 @@
             device_id_type=MESH_IDS,
         )
 
+    def load(source, target, sem):
+        copy = pltpu.make_async_copy(source, target, sem)
+        copy.start()
+        return copy
+
+    token_load = load(tokens_hbm, tokens, small_sem.at[0])
+    gain_load = load(attn_gain_hbm, attn_gain, small_sem.at[1])
+    query_load = load(w_query_hbm, w_query, small_sem.at[2])
+    cache_loads = []
+    for number, (source, target) in enumerate(((key_hbm, keys), (value_hbm, values))):
+        for half in reversed(range(2)):
+            part = pl.ds(half * (cache_len // 2), cache_len // 2)
+            for third in range(2):
+                seqs = pl.ds(third * pairs, pairs)
+                pltpu.make_async_copy(
+                    source.at[seqs, :, part],
+                    target.at[seqs, :, part],
+                    pair_sem.at[2 * number + 1 - half],
+                ).start()
+            whole = target.at[:, :, part]
+            cache_loads.append(
+                pltpu.make_async_copy(whole, whole, pair_sem.at[2 * number + 1 - half])
+            )
+        if number == 0:
+            for step in range(n_ep - 1):
+                greet(far_ep(step), tp)
+            for peer_tp in tp_order[:-1]:
+                greet(ep, peer_tp)
+            length_load = load(lengths_hbm, lengths, small_sem.at[3])
+            bias_load = load(head_bias_hbm, head_bias, small_sem.at[4])
+    own_loads = [
+        load(w_key_hbm, w_key, small_sem.at[5]),
+        load(w_value_hbm, w_value, small_sem.at[9]),
+    ]
+    out_load = load(w_out_hbm, w_out, weight_sem.at[0])
+    route_loads = [
+        load(ffn_gain_hbm, ffn_gain, small_sem.at[6]),
+        load(route_ids_hbm, route_ids, small_sem.at[7]),
+        load(route_weights_hbm, route_weights, small_sem.at[8]),
+    ]
+    weight_loads = [
+        load(w_gate_hbm, w_gate, weight_sem.at[1]),
+        load(w_up_hbm, w_up, weight_sem.at[2]),
+        load(w_down_hbm, w_down, weight_sem.at[3]),
+    ]
     ffn_rows[...] = jnp.zeros_like(ffn_rows)
-    each_peer(greet)
-
-    small = []
-    for number, (source, target) in enumerate(
-        (
-            (tokens_hbm, tokens),
-            (attn_gain_hbm, attn_gain),
-            (w_query_hbm, w_query),
-            (w_key_hbm, w_key),
-            (w_value_hbm, w_value),
-            (lengths_hbm, lengths),
-            (head_bias_hbm, head_bias),
-            (ffn_gain_hbm, ffn_gain),
-            (route_ids_hbm, route_ids),
-            (route_weights_hbm, route_weights),
-        )
-    ):
-        copy = pltpu.make_async_copy(source, target, small_sem.at[number])
-        if number not in (3, 4):
-            copy.start()
-        small.append(copy)
-    key_copies, value_copies, weight_copies = [], [], []
-    for pair in range(pairs):
-        part = pl.ds(2 * pair, 2)
-        copy = pltpu.make_async_copy(key_hbm.at[part], keys.at[part], pair_sem.at[pair])
-        copy.start()
-        key_copies.append(copy)
-    for pair in range(pairs):
-        part = pl.ds(2 * pair, 2)
-        copy = pltpu.make_async_copy(
-            value_hbm.at[part], values.at[part], pair_sem.at[pairs + pair]
-        )
-        copy.start()
-        value_copies.append(copy)
-    small[3].start()
-    small[4].start()
-    for number, (source, target) in enumerate(
-        (
-            (w_out_hbm, w_out),
-            (w_gate_hbm, w_gate),
-            (w_up_hbm, w_up),
-            (w_down_hbm, w_down),
-        )
-    ):
-        copy = pltpu.make_async_copy(source, target, weight_sem.at[number])
-        copy.start()
-        weight_copies.append(copy)
 
     block_len = 256 if cache_len % 256 == 0 else 128
     n_blocks = cache_len // block_len
@@ -178,60 +176,47 @@
         iota((block_len, block_len), 0) > iota((block_len, block_len), 1)
     ).astype(BF16)
     flat = rows * heads
-    expand = (iota((flat, ROW_TILE), 0) // heads == iota((flat, ROW_TILE), 1)).astype(BF16)
-    collapse = (iota((ROW_TILE, flat), 1) // heads == iota((ROW_TILE, flat), 0)).astype(BF16)
-    own_head = iota((flat, query_cols), 1) // HEAD_SIZE == lax.rem(
-        iota((flat, query_cols), 0), heads
-    )
-    fold_row = iota((query_cols, key_cols), 0)
-    fold_col = iota((query_cols, key_cols), 1)
-    fold = (
-        (fold_row // (HEAD_SIZE * group)) * HEAD_SIZE + lax.rem(fold_row, HEAD_SIZE)
-        == fold_col
-    ).astype(BF16)
-    unfold_row = iota((key_cols, query_cols), 0)
-    unfold_col = iota((key_cols, query_cols), 1)
-    unfold = (
-        (unfold_col // (HEAD_SIZE * group)) * HEAD_SIZE + lax.rem(unfold_col, HEAD_SIZE)
-        == unfold_row
-    ).astype(BF16)
-    odd = lax.rem(iota((flat, key_cols), 0) // heads, 2) == 1
-
-    small[0].wait()
-    token_rows[...] = jnp.zeros_like(token_rows)
-    token_rows[:rows, :] = tokens[...].astype(F32)
-    rows_f32 = token_rows[...]
-    small[1].wait()
+    seq_col = lax.rem(iota((flat, 1), 0), rows)
+    head_col = iota((flat, 1), 0) // rows
+
+    token_load.wait()
+    rows_f32 = tokens[...].astype(F32)
+    gain_load.wait()
     normed = (
         rows_f32
         * lax.rsqrt(jnp.mean(rows_f32 * rows_f32, axis=1, keepdims=True) + EPSILON)
         * attn_gain[...]
     ).astype(BF16)
-    small[2].wait()
-    queries = dot(normed, w_query[...]).astype(BF16)
-    spread = jnp.where(own_head, dot(expand, queries), 0.0).astype(BF16)
-    folded = dot(spread, fold)
-    left = jnp.where(odd, 0.0, folded).astype(BF16)
-    right = jnp.where(odd, folded, 0.0).astype(BF16)
-
-    small[5].wait()
-    small[6].wait()
-    row_col = iota((flat, 1), 0)
+    query_load.wait()
+    queries = dot(normed, w_query[...]).astype(BF16).astype(F32)
+    for head in range(heads):
+        first = head // group * HEAD_SIZE
+        piece = queries[:, head * HEAD_SIZE : (head + 1) * HEAD_SIZE]
+        sides = [jnp.zeros((rows, first), F32)] if first else []
+        sides.append(piece)
+        if key_cols > first + HEAD_SIZE:
+            sides.append(jnp.zeros((rows, key_cols - first - HEAD_SIZE), F32))
+        spread[head * rows : (head + 1) * rows, :] = jnp.concatenate(sides, axis=1)
+    folded = spread[...].astype(BF16)
+    query_block = jnp.where(
+        iota((flat, rows * key_cols), 1) // key_cols == seq_col,
+        jnp.concatenate([folded] * rows, axis=1),
+        0.0,
+    ).astype(BF16)
+
+    length_load.wait()
+    bias_load.wait()
     length_col = jnp.zeros((flat, 1), jnp.int32)
     for row in range(rows):
-        length_col = jnp.where(row_col // heads == row, lengths[row], length_col)
+        length_col = jnp.where(seq_col == row, lengths[row], length_col)
     bias_col = jnp.zeros((flat, 1), F32)
     for head in range(heads):
-        bias_col = jnp.where(lax.rem(row_col, heads) == head, head_bias[head], bias_col)
-    pieces = []
-    for pair in range(pairs):
-        key_copies[pair].wait()
-        part = slice(2 * heads * pair, 2 * heads * (pair + 1))
-        block = keys[2 * pair : 2 * pair + 2].reshape(2 * key_cols, cache_len)
-        query_block = jnp.concatenate([left[part], right[part]], axis=1)
-        pieces.append(dot(query_block, block))
-    scores = jnp.concatenate(pieces, axis=0) * HEAD_SIZE ** (-0.5) + bias_col
-
+        bias_col = jnp.where(head_col == head, head_bias[head], bias_col)
+
+    for copy in cache_loads[:2]:
+        copy.wait()
+    key_rows = keys[...].reshape(rows * key_cols, cache_len)
+    scores = dot(query_block, key_rows) * HEAD_SIZE ** (-0.5) + bias_col
     in_cache = iota((flat, cache_len), 1) < length_col
     soft = jnp.log(1.0 + jnp.exp(-jnp.abs(scores)))
     log_rest = jnp.where(in_cache, jnp.minimum(-scores, 0.0) - soft, 0.0)
@@ -250,30 +235,38 @@
     carried = jnp.zeros((flat, 1), F32)
     tails = [None] * n_blocks
     for block in reversed(range(n_blocks)):
-        inner = (
+        tails[block] = (
             within[block * flat : (block + 1) * flat]
             + within[(n_blocks + block) * flat : (n_blocks + block + 1) * flat]
+            + carried
         )
-        tails[block] = inner + carried
-        first = block * block_len
-        carried = carried + inner[:, :1] + log_rest[:, first : first + 1]
+        part = log_rest[:, block * block_len : (block + 1) * block_len]
+        carried = carried + jnp.sum(part, axis=1, keepdims=True)
     tail_sum = jnp.concatenate(tails, axis=1)
     breaks = jnp.where(in_cache, jnp.exp(log_take + tail_sum), 0.0).astype(BF16)
-
-    for copy in value_copies:
+    for copy in cache_loads[2:]:
         copy.wait()
     value_rows = values[...].reshape(rows * key_cols, cache_len)
-    crossed = dot(value_rows, breaks.T).T
+    crossed = lax.dot_general(
+        breaks, value_rows, (((1,), (1,)), ((), ())), preferred_element_type=F32
+    )
     own = jnp.zeros((flat, key_cols), F32)
     for row in range(rows):
-        part = slice(row * key_cols, (row + 1) * key_cols)
-        own = jnp.where(row_col // heads == row, crossed[:, part], own)
-    own = own.astype(BF16)
-    unfolded = jnp.where(own_head, dot(own, unfold), 0.0).astype(BF16)
-    heads_out = dot(collapse, unfolded).astype(BF16)
-
-    pl.semaphore_wait(barrier, n_peers - 1)
-    head_part[...] = heads_out[:rows]
+        own = jnp.where(seq_col == row, crossed[:, row * key_cols : (row + 1) * key_cols], own)
+    spread[...] = own
+    heads_out = jnp.concatenate(
+        [
+            spread[
+                head * rows : (head + 1) * rows,
+                head // group * HEAD_SIZE : (head // group + 1) * HEAD_SIZE,
+            ]
+            for head in range(heads)
+        ],
+        axis=1,
+    ).astype(BF16)
+
+    pl.semaphore_wait(barrier, n_ep + n_tp - 2)
+    head_part[...] = heads_out
     own_cols = pl.ds(pl.multiple_of(tp * query_cols, query_cols), query_cols)
     head_slot = head_all.at[:, own_cols]
     for peer_tp in tp_order[:-1]:
@@ -286,16 +279,16 @@
             device_id_type=MESH_IDS,
         ).start()
     pltpu.make_async_copy(head_part, head_slot, recv_sem.at[0]).start()
-    small[3].wait()
-    small[4].wait()
-    new_keys_ref[...] = dot(normed, w_key[...]).astype(BF16)[:rows]
-    new_values_ref[...] = dot(normed, w_value[...]).astype(BF16)[:rows]
-    weight_copies[0].wait()
+    for copy in own_loads:
+        copy.wait()
+    new_keys_ref[...] = dot(normed, w_key[...]).astype(BF16)
+    new_values_ref[...] = dot(normed, w_value[...]).astype(BF16)
+    out_load.wait()
     pltpu.make_async_copy(head_all, head_all, recv_sem.at[0]).wait()
     attn_out = dot(head_all[...], w_out[...])
 
     slice_cols = pl.ds(pl.multiple_of(tp * slice_width, slice_width), slice_width)
-    own_hidden = token_rows[:rows, slice_cols] + attn_out
+    own_hidden = tokens[:, slice_cols].astype(F32) + attn_out
     hidden_part[...] = own_hidden.astype(BF16)
     hidden_slot = hidden_all.at[ep, :, slice_cols]
 
@@ -311,7 +304,7 @@
 
     each_peer(send_hidden)
     pltpu.make_async_copy(hidden_part, hidden_slot, recv_sem.at[1]).start()
-    for copy in small[7:]:
+    for copy in route_loads:
         copy.wait()
     diagonal = iota((rows, rows), 0) == iota((rows, rows), 1)
     choices = []
@@ -324,7 +317,7 @@
                 for row in (id_row, weight_row)
             )
         )
-    for copy in weight_copies[1:]:
+    for copy in weight_loads:
         copy.wait()
     pltpu.make_async_copy(hidden_all, hidden_all, recv_sem.at[1]).wait()
     for source in range(n_ep):
@@ -454,7 +447,7 @@
     ]
     n_peers = n_ep * n_tp
     scratch = buffers + [
-        pltpu.VMEM((ROW_TILE, width), F32),
+        pltpu.VMEM((rows * (query_cols // HEAD_SIZE), key_cols), F32),
         pltpu.VMEM((rows, query_cols), BF16),
         pltpu.VMEM((rows, query_cols * n_tp), BF16),
         pltpu.VMEM((rows, slice_width), BF16),
@@ -463,7 +456,7 @@
         pltpu.VMEM((n_tp, n_ep, rows, slice_width), BF16),
         pltpu.VMEM((n_peers, rows, slice_width), BF16),
         pltpu.SemaphoreType.DMA((10,)),
-        pltpu.SemaphoreType.DMA((rows,)),
+        pltpu.SemaphoreType.DMA((4,)),
         pltpu.SemaphoreType.DMA((4,)),
         pltpu.SemaphoreType.DMA((3,)),
         pltpu.SemaphoreType.DMA((3,)),

time: 23.1 us -> 22.5 us (0.974)
  Pallas kernels: 22.3 us -> 21.7 us
    pallas_call x1, Pallas kernels: 21.6 us -> 21 us  [shards(): pl.pallas_call(functools.partial(layer_kernel, n_ep, n_tp), out_shape=(pl...]
where the time goes in v1:
time: 22.5 us; the launch traced here: 22.3 us
  Pallas kernels  21.7 us (96%)
  between operations  0.65 us (3%)
    pallas_call x1, Pallas kernels, shards(): pl.pallas_call(functools.partial(layer_kernel, n_ep, n_tp), out_shape=(pl...  21 us
    pallas_call x1, Pallas kernels, shards(): pl.pallas_call(place_results, out_shape=tuple((jax.ShapeDtypeStruct(r.sha...  0.63 us

profile of v1, /device:TPU:0, one launch (start us, length us, event | category | flops | bytes accessed | tf_op | source)
XLA Modules:
  0.0 22.3 jit_solution(17951816165713604243)
XLA Ops:
  0.6 21.0 %layer.1 = (bf16[10,256]{1,0:T(8,128)(2,1)S(1)}, bf16[10,128]{1,0:T(8,128)(2,1)S(1)}, bf16[10,128]{1,0:T(8,128)(2,1)S(1)}) custom-call(bf16[10,1024]{1,0:T(8,128)(2,1)} %tokens_hbm.1, f32[1,1024]{1,0:T(1,128)} %bitcast.4, bf16[1024,256]{1,0:T(8,128)(2,1)} %w_query_hbm.1, bf16[1024,128]{1,0:T(8,128)(2,1)} %w_key_hbm.1, bf16[1024,128]{1,0:T(8,128)(2,1)} %w_value_hbm.1, ...), custom_call_target="tpu_custom_call" | custom-call | tf_op jit(solution)/shard_map/layer/pallas_call | solution.py:464
  21.7 0.6 %place.1 = (bf16[10,256]{1,0:T(8,128)(2,1)}, bf16[10,128]{1,0:T(8,128)(2,1)}, bf16[10,128]{1,0:T(8,128)(2,1)}) custom-call(bf16[10,256]{1,0:T(8,128)(2,1)S(1)} %get-tuple-element.6.refs_0_, bf16[10,128]{1,0:T(8,128)(2,1)S(1)} %get-tuple-element.7.refs_1_, bf16[10,128]{1,0:T(8,128)(2,1)S(1)} %get-tuple-element.8.refs_2_), custom_call_target="tpu_custom_call" | custom-call | tf_op jit(solution)/shard_map/place/pallas_call | solution.py:479

commit v2 on v1

--- a/solution.py
+++ b/solution.py
@@ -26,6 +26,7 @@
 def layer_kernel(
     n_ep,
     n_tp,
+    n_messages,
     tokens_hbm,
     attn_gain_hbm,
     w_query_hbm,
@@ -58,15 +59,14 @@
     ffn_gain,
     route_ids,
     route_weights,
-    w_gate,
-    w_up,
+    w_in,
     w_down,
     spread,
     head_part,
     head_all,
     hidden_part,
     hidden_all,
-    ffn_rows,
+    hidden_rows,
     out_parts,
     returned,
     small_sem,
@@ -77,8 +77,6 @@
 ):
     ep = lax.axis_index("ep")
     tp = lax.axis_index("tp")
-    me = ep * n_tp + tp
-    n_peers = n_ep * n_tp
     rows = tokens.shape[0]
     query_cols = w_query.shape[1]
     key_cols = w_key_hbm.shape[1]
@@ -100,18 +98,29 @@
     tp_order = [other_tp(step) for step in range(n_tp - 2)]
     tp_order += [other_tp(n_tp - 1), tp]
 
-    def each_peer(fn):
-        def to_ep(step):
-            for peer_tp in tp_order:
-                fn(far_ep(step), peer_tp)
-
-        if n_peers <= 16:
-            for step in range(n_ep - 1):
-                to_ep(step)
+    share = n_ep * n_tp // n_messages
+    half, chips = n_ep // share, n_tp // share
+    side, chip, keeper = lax.rem(tp, share), tp // share, ep // half
+    first_ep = side * half
+    mine = keeper == side
+    other_chips = [lax.rem(chip + 1 + step, chips) for step in range(chips - 1)]
+
+    def copy_to(source, target, number, peer_ep, peer_tp):
+        pltpu.make_async_remote_copy(
+            src_ref=source,
+            dst_ref=target,
+            send_sem=send_sem.at[number],
+            recv_sem=recv_sem.at[number],
+            device_id={"ep": peer_ep, "tp": peer_tp},
+            device_id_type=MESH_IDS,
+        ).start()
+
+    def repeat(count, fn):
+        if count <= 4:
+            for step in range(count):
+                fn(step)
         else:
-            pl.loop(0, n_ep - 1)(to_ep)
-        for peer_tp in tp_order[:-1]:
-            fn(ep, peer_tp)
+            pl.loop(0, count)(fn)
 
     barrier = pltpu.get_barrier_semaphore()
 
@@ -133,18 +142,18 @@
     query_load = load(w_query_hbm, w_query, small_sem.at[2])
     cache_loads = []
     for number, (source, target) in enumerate(((key_hbm, keys), (value_hbm, values))):
-        for half in reversed(range(2)):
-            part = pl.ds(half * (cache_len // 2), cache_len // 2)
+        for upper in reversed(range(2)):
+            part = pl.ds(upper * (cache_len // 2), cache_len // 2)
             for third in range(2):
                 seqs = pl.ds(third * pairs, pairs)
                 pltpu.make_async_copy(
                     source.at[seqs, :, part],
                     target.at[seqs, :, part],
-                    pair_sem.at[2 * number + 1 - half],
+                    pair_sem.at[2 * number + 1 - upper],
                 ).start()
             whole = target.at[:, :, part]
             cache_loads.append(
-                pltpu.make_async_copy(whole, whole, pair_sem.at[2 * number + 1 - half])
+                pltpu.make_async_copy(whole, whole, pair_sem.at[2 * number + 1 - upper])
             )
         if number == 0:
             for step in range(n_ep - 1):
@@ -164,11 +173,11 @@
         load(route_weights_hbm, route_weights, small_sem.at[8]),
     ]
     weight_loads = [
-        load(w_gate_hbm, w_gate, weight_sem.at[1]),
-        load(w_up_hbm, w_up, weight_sem.at[2]),
-        load(w_down_hbm, w_down, weight_sem.at[3]),
+        load(w_gate_hbm.at[0], w_in.at[0, 0], weight_sem.at[1]),
+        load(w_up_hbm.at[0], w_in.at[0, 1], weight_sem.at[2]),
+        load(w_down_hbm.at[0], w_down.at[0], weight_sem.at[3]),
     ]
-    ffn_rows[...] = jnp.zeros_like(ffn_rows)
+    hidden_rows[...] = jnp.zeros_like(hidden_rows)
 
     block_len = 256 if cache_len % 256 == 0 else 128
     n_blocks = cache_len // block_len
@@ -270,15 +279,13 @@
     own_cols = pl.ds(pl.multiple_of(tp * query_cols, query_cols), query_cols)
     head_slot = head_all.at[:, own_cols]
     for peer_tp in tp_order[:-1]:
-        pltpu.make_async_remote_copy(
-            src_ref=head_part,
-            dst_ref=head_slot,
-            send_sem=send_sem.at[0],
-            recv_sem=recv_sem.at[0],
-            device_id={"tp": peer_tp},
-            device_id_type=MESH_IDS,
-        ).start()
+        copy_to(head_part, head_slot, 0, ep, peer_tp)
     pltpu.make_async_copy(head_part, head_slot, recv_sem.at[0]).start()
+    partner = tp + 1 - 2 * side
+    for copy in weight_loads:
+        copy.wait()
+    if share == 2:
+        copy_to(w_in.at[0], w_in.at[1], 3, ep, partner)
     for copy in own_loads:
         copy.wait()
     new_keys_ref[...] = dot(normed, w_key[...]).astype(BF16)
@@ -289,21 +296,30 @@
 
     slice_cols = pl.ds(pl.multiple_of(tp * slice_width, slice_width), slice_width)
     own_hidden = tokens[:, slice_cols].astype(F32) + attn_out
-    hidden_part[...] = own_hidden.astype(BF16)
-    hidden_slot = hidden_all.at[ep, :, slice_cols]
-
-    def send_hidden(peer_ep, peer_tp):
-        pltpu.make_async_remote_copy(
-            src_ref=hidden_part,
-            dst_ref=hidden_slot,
-            send_sem=send_sem.at[1],
-            recv_sem=recv_sem.at[1],
-            device_id={"ep": peer_ep, "tp": peer_tp},
-            device_id_type=MESH_IDS,
-        ).start()
-
-    each_peer(send_hidden)
-    pltpu.make_async_copy(hidden_part, hidden_slot, recv_sem.at[1]).start()
+    rounded = own_hidden.astype(BF16)
+    for pair in range(pairs):
+        hidden_part[pair] = rounded[2 * pair : 2 * pair + 2]
+    hidden_slot = hidden_all.at[lax.rem(ep, half), tp]
+
+    def send_hidden(step):
+        for peer_chip in other_chips + [chip]:
+            copy_to(hidden_part, hidden_slot, 1, far_ep(step), peer_chip * share + keeper)
+
+    repeat(n_ep - 1, send_hidden)
+    for peer_chip in other_chips:
+        copy_to(hidden_part, hidden_slot, 1, ep, peer_chip * share + keeper)
+
+    @pl.when(mine)
+    def _():
+        pltpu.make_async_copy(hidden_part, hidden_slot, recv_sem.at[1]).start()
+
+    if share == 2:
+
+        @pl.when(jnp.logical_not(mine))
+        def _():
+            copy_to(hidden_part, hidden_slot, 1, ep, partner)
+
+        copy_to(w_down.at[0], w_down.at[1], 4, ep, partner)
     for copy in route_loads:
         copy.wait()
     diagonal = iota((rows, rows), 0) == iota((rows, rows), 1)
@@ -317,63 +333,70 @@
                 for row in (id_row, weight_row)
             )
         )
-    for copy in weight_loads:
-        copy.wait()
+    if share == 2:
+        pltpu.make_async_copy(w_in.at[1], w_in.at[1], recv_sem.at[3]).wait()
     pltpu.make_async_copy(hidden_all, hidden_all, recv_sem.at[1]).wait()
-    for source in range(n_ep):
-        hidden = hidden_all[source].astype(F32)
-        first = source * ROW_TILE
-        ffn_rows[first : first + rows, :] = (
-            hidden
-            * lax.rsqrt(jnp.mean(hidden * hidden, axis=1, keepdims=True) + EPSILON)
-            * ffn_gain[...]
-        ).astype(BF16)
-    ffn_in = ffn_rows[...]
-
-    gate_act = dot(ffn_in, w_gate[0])
-    up_act = dot(ffn_in, w_up[0])
-    hidden_act = (gate_act / (1.0 + jnp.exp(-gate_act)) * up_act).astype(BF16)
-    for step in range(n_tp):
-        to_tp = tp_order[step]
-        part = pl.ds(pl.multiple_of(to_tp * slice_width, slice_width), slice_width)
-        partial_out = dot(hidden_act, w_down[0, :, part]).astype(BF16)
-        for owner in range(n_ep):
-            first = owner * ROW_TILE
-            out_parts[step, owner] = partial_out[first : first + rows]
-
-        def send_out(to_ep):
-            pltpu.make_async_remote_copy(
-                src_ref=out_parts.at[step, to_ep],
-                dst_ref=returned.at[me],
-                send_sem=send_sem.at[2],
-                recv_sem=recv_sem.at[2],
-                device_id={"ep": to_ep, "tp": to_tp},
-                device_id_type=MESH_IDS,
-            ).start()
-
-        if n_ep <= 8:
-            for hop in range(n_ep - 1):
-                send_out(far_ep(hop))
-        else:
-
-            @pl.loop(0, n_ep - 1)
-            def _(hop):
-                send_out(far_ep(hop))
-
-        if step < n_tp - 1:
-            send_out(ep)
-        else:
-            pltpu.make_async_copy(
-                out_parts.at[step, ep],
-                returned.at[me],
-                recv_sem.at[2],
-            ).start()
+    for source in range(half):
+        for peer_tp in range(n_tp):
+            part = slice(peer_tp * slice_width, (peer_tp + 1) * slice_width)
+            for pair in range(pairs):
+                first = source * ROW_TILE + 2 * pair
+                hidden_rows[first : first + 2, part] = hidden_all[
+                    source, peer_tp, pair
+                ].astype(F32)
+    hidden = hidden_rows[...]
+    scaled = (hidden * ffn_gain[...]).astype(BF16)
+    row_scale = lax.rsqrt(jnp.mean(hidden * hidden, axis=1, keepdims=True) + EPSILON)
+    acts = []
+    for member in range(share):
+        gate_act = dot(scaled, w_in[member, 0]) * row_scale
+        up_act = dot(scaled, w_in[member, 1]) * row_scale
+        acts.append((gate_act / (1.0 + jnp.exp(-gate_act)) * up_act).astype(BF16))
+    hidden_act = jnp.concatenate(acts, axis=1)
+    if share == 2:
+        pltpu.make_async_copy(w_down.at[1], w_down.at[1], recv_sem.at[4]).wait()
+    expert_rows = dot(hidden_act, w_down[...].reshape(hidden_act.shape[1], -1)).astype(BF16)
+    for source in range(half):
+        for peer_tp in range(n_tp):
+            part = slice(peer_tp * slice_width, (peer_tp + 1) * slice_width)
+            for pair in range(pairs):
+                first = source * ROW_TILE + 2 * pair
+                out_parts[peer_tp, source, pair] = expert_rows[first : first + 2, part]
+    out_slot = returned.at[ep * chips + chip]
+
+    def far_owner(step):
+        return jnp.where(2 * ep >= 2 * first_ep + half, step, half - 1 - step)
+
+    def send_out(step):
+        source = far_owner(step)
+        for peer_tp in tp_order[:-1]:
+            copy_to(out_parts.at[peer_tp, source], out_slot, 2, first_ep + source, peer_tp)
+
+    def send_own(step):
+        source = far_owner(step)
+
+        @pl.when(first_ep + source != ep)
+        def _():
+            copy_to(out_parts.at[tp, source], out_slot, 2, first_ep + source, tp)
+
+        @pl.when(first_ep + source == ep)
+        def _():
+            pltpu.make_async_copy(out_parts.at[tp, source], out_slot, recv_sem.at[2]).start()
+
+    repeat(half, send_out)
+    repeat(half, send_own)
     pltpu.make_async_copy(returned, returned, recv_sem.at[2]).wait()
+
+    def expert_part(number):
+        return jnp.concatenate(
+            [returned[number, pair].astype(F32) for pair in range(pairs)], axis=0
+        )
+
     mixed = own_hidden
     for expert in range(n_ep):
-        total = returned[expert * n_tp].astype(F32)
-        for number in range(1, n_tp):
-            total = total + returned[expert * n_tp + number].astype(F32)
+        total = expert_part(expert * chips)
+        for number in range(1, chips):
+            total = total + expert_part(expert * chips + number)
         scale = jnp.zeros((rows, 1), F32)
         for id_col, weight_col in choices:
             scale = scale + jnp.where(id_col == expert, weight_col, 0.0)
@@ -382,9 +405,20 @@
 
     sent = head_all.at[:, pl.ds(0, (n_tp - 1) * query_cols)]
     pltpu.make_async_copy(sent, sent, send_sem.at[0]).wait()
-    sent = returned.at[pl.ds(0, n_peers - 1)]
-    pltpu.make_async_copy(sent, sent, send_sem.at[1]).wait()
-    pltpu.make_async_copy(sent, sent, send_sem.at[2]).wait()
+    for number in (1, 2):
+
+        @pl.when(mine)
+        def _():
+            sent = returned.at[pl.ds(0, n_messages - 1)]
+            pltpu.make_async_copy(sent, sent, send_sem.at[number]).wait()
+
+        @pl.when(jnp.logical_not(mine))
+        def _():
+            pltpu.make_async_copy(returned, returned, send_sem.at[number]).wait()
+
+    if share == 2:
+        pltpu.make_async_copy(w_in.at[1], w_in.at[1], send_sem.at[3]).wait()
+        pltpu.make_async_copy(w_down.at[1], w_down.at[1], send_sem.at[4]).wait()
 
 
 def place_results(*refs):
@@ -443,26 +477,31 @@
     in_smem = (7, 8)
     buffers = [
         (pltpu.SMEM if number in in_smem else pltpu.VMEM)(operand.shape, operand.dtype)
-        for number, operand in enumerate(operands)
+        for number, operand in enumerate(operands[:13])
     ]
-    n_peers = n_ep * n_tp
+    share = 2 if n_ep % 2 == 0 and n_tp % 2 == 0 else 1
+    half, pairs = n_ep // share, rows // 2
+    n_messages = half * n_tp
+    hidden_units = w_gate.shape[2]
     scratch = buffers + [
+        pltpu.VMEM((share, 2, width, hidden_units), BF16),
+        pltpu.VMEM((share, hidden_units, width), BF16),
         pltpu.VMEM((rows * (query_cols // HEAD_SIZE), key_cols), F32),
         pltpu.VMEM((rows, query_cols), BF16),
         pltpu.VMEM((rows, query_cols * n_tp), BF16),
-        pltpu.VMEM((rows, slice_width), BF16),
-        pltpu.VMEM((n_ep, rows, width), BF16),
-        pltpu.VMEM((n_ep * ROW_TILE, width), BF16),
-        pltpu.VMEM((n_tp, n_ep, rows, slice_width), BF16),
-        pltpu.VMEM((n_peers, rows, slice_width), BF16),
+        pltpu.VMEM((pairs, 2, slice_width), BF16),
+        pltpu.VMEM((half, n_tp, pairs, 2, slice_width), BF16),
+        pltpu.VMEM((half * ROW_TILE, width), F32),
+        pltpu.VMEM((n_tp, half, pairs, 2, slice_width), BF16),
+        pltpu.VMEM((n_messages, pairs, 2, slice_width), BF16),
         pltpu.SemaphoreType.DMA((10,)),
         pltpu.SemaphoreType.DMA((4,)),
         pltpu.SemaphoreType.DMA((4,)),
-        pltpu.SemaphoreType.DMA((3,)),
-        pltpu.SemaphoreType.DMA((3,)),
+        pltpu.SemaphoreType.DMA((5,)),
+        pltpu.SemaphoreType.DMA((5,)),
     ]
     results = pl.pallas_call(
-        functools.partial(layer_kernel, n_ep, n_tp),
+        functools.partial(layer_kernel, n_ep, n_tp, n_messages),
         out_shape=(
             pltpu.VMEM((rows, slice_width), BF16),
             pltpu.VMEM((rows, key_cols), BF16),

time: 22.5 us -> 20.7 us (0.920)
  Pallas kernels: 21.7 us -> 19.9 us
    pallas_call x1, Pallas kernels: 21 us -> 19.3 us  [shards(): pl.pallas_call(functools.partial(layer_kernel, n_ep, n_tp, n_messages), o...]
where the time goes in v2:
time: 20.7 us; the launch traced here: 20.6 us
  Pallas kernels  19.9 us (96%)
  between operations  0.65 us (3%)
    pallas_call x1, Pallas kernels, shards(): pl.pallas_call(functools.partial(layer_kernel, n_ep, n_tp, n_messages), o...  19.3 us
    pallas_call x1, Pallas kernels, shards(): pl.pallas_call(place_results, out_shape=tuple((jax.ShapeDtypeStruct(r.sha...  0.63 us

profile of v2, /device:TPU:0, one launch (start us, length us, event | category | flops | bytes accessed | tf_op | source)
XLA Modules:
  0.0 20.6 jit_solution(14321986542929850438)
XLA Ops:
  0.6 19.3 %layer.1 = (bf16[10,256]{1,0:T(8,128)(2,1)S(1)}, bf16[10,128]{1,0:T(8,128)(2,1)S(1)}, bf16[10,128]{1,0:T(8,128)(2,1)S(1)}) custom-call(bf16[10,1024]{1,0:T(8,128)(2,1)} %tokens_hbm.1, f32[1,1024]{1,0:T(1,128)} %bitcast.4, bf16[1024,256]{1,0:T(8,128)(2,1)} %w_query_hbm.1, bf16[1024,128]{1,0:T(8,128)(2,1)} %w_key_hbm.1, bf16[1024,128]{1,0:T(8,128)(2,1)} %w_value_hbm.1, ...), custom_call_target="tpu_custom_call" | custom-call | tf_op jit(solution)/shard_map/layer/pallas_call | solution.py:503
  19.9 0.6 %place.1 = (bf16[10,256]{1,0:T(8,128)(2,1)}, bf16[10,128]{1,0:T(8,128)(2,1)}, bf16[10,128]{1,0:T(8,128)(2,1)}) custom-call(bf16[10,256]{1,0:T(8,128)(2,1)S(1)} %get-tuple-element.6.refs_0_, bf16[10,128]{1,0:T(8,128)(2,1)S(1)} %get-tuple-element.7.refs_1_, bf16[10,128]{1,0:T(8,128)(2,1)S(1)} %get-tuple-element.8.refs_2_), custom_call_target="tpu_custom_call" | custom-call | tf_op jit(solution)/shard_map/place/pallas_call | solution.py:518

commit v3 on v2

--- a/solution.py
+++ b/solution.py
@@ -100,8 +100,8 @@
 
     share = n_ep * n_tp // n_messages
     half, chips = n_ep // share, n_tp // share
-    side, chip, keeper = lax.rem(tp, share), tp // share, ep // half
-    first_ep = side * half
+    side, chip, keeper = lax.rem(tp, share), tp // share, share - 1 - ep // half
+    first_ep = (share - 1 - side) * half
     mine = keeper == side
     other_chips = [lax.rem(chip + 1 + step, chips) for step in range(chips - 1)]
 
@@ -140,28 +140,40 @@
     token_load = load(tokens_hbm, tokens, small_sem.at[0])
     gain_load = load(attn_gain_hbm, attn_gain, small_sem.at[1])
     query_load = load(w_query_hbm, w_query, small_sem.at[2])
-    cache_loads = []
-    for number, (source, target) in enumerate(((key_hbm, keys), (value_hbm, values))):
-        for upper in reversed(range(2)):
-            part = pl.ds(upper * (cache_len // 2), cache_len // 2)
-            for third in range(2):
-                seqs = pl.ds(third * pairs, pairs)
-                pltpu.make_async_copy(
-                    source.at[seqs, :, part],
-                    target.at[seqs, :, part],
-                    pair_sem.at[2 * number + 1 - upper],
-                ).start()
-            whole = target.at[:, :, part]
-            cache_loads.append(
-                pltpu.make_async_copy(whole, whole, pair_sem.at[2 * number + 1 - upper])
-            )
-        if number == 0:
-            for step in range(n_ep - 1):
-                greet(far_ep(step), tp)
-            for peer_tp in tp_order[:-1]:
-                greet(ep, peer_tp)
-            length_load = load(lengths_hbm, lengths, small_sem.at[3])
-            bias_load = load(head_bias_hbm, head_bias, small_sem.at[4])
+    def load_cache(source, target, sem):
+        for pair in range(pairs):
+            part = pl.ds(2 * pair, 2)
+            pltpu.make_async_copy(source.at[part], target.at[part], sem).start()
+        return pltpu.make_async_copy(target, target, sem)
+
+    key_load = load_cache(key_hbm, keys, pair_sem.at[0])
+    for step in range(n_ep - 1):
+        greet(far_ep(step), tp)
+    for peer_tp in tp_order[:-1]:
+        greet(ep, peer_tp)
+    value_load = load_cache(value_hbm, values, pair_sem.at[1])
+    length_load = load(lengths_hbm, lengths, small_sem.at[3])
+    bias_load = load(head_bias_hbm, head_bias, small_sem.at[4])
+    hidden_rows[...] = jnp.zeros_like(hidden_rows)
+
+    block_len = 256 if cache_len % 256 == 0 else 128
+    n_blocks = cache_len // block_len
+    triangle = (
+        iota((block_len, block_len), 0) > iota((block_len, block_len), 1)
+    ).astype(BF16)
+    flat = rows * heads
+    seq_col = lax.rem(iota((flat, 1), 0), rows)
+    head_col = iota((flat, 1), 0) // rows
+
+    token_load.wait()
+    rows_f32 = tokens[...].astype(F32)
+    gain_load.wait()
+    normed = (
+        rows_f32
+        * lax.rsqrt(jnp.mean(rows_f32 * rows_f32, axis=1, keepdims=True) + EPSILON)
+        * attn_gain[...]
+    ).astype(BF16)
+    query_load.wait()
     own_loads = [
         load(w_key_hbm, w_key, small_sem.at[5]),
         load(w_value_hbm, w_value, small_sem.at[9]),
@@ -172,31 +184,12 @@
         load(route_ids_hbm, route_ids, small_sem.at[7]),
         load(route_weights_hbm, route_weights, small_sem.at[8]),
     ]
+    for number, source in enumerate((w_gate_hbm, w_up_hbm)):
+        pltpu.make_async_copy(source.at[0], w_in.at[0, number], weight_sem.at[1]).start()
     weight_loads = [
-        load(w_gate_hbm.at[0], w_in.at[0, 0], weight_sem.at[1]),
-        load(w_up_hbm.at[0], w_in.at[0, 1], weight_sem.at[2]),
-        load(w_down_hbm.at[0], w_down.at[0], weight_sem.at[3]),
+        pltpu.make_async_copy(w_in.at[0], w_in.at[0], weight_sem.at[1]),
+        load(w_down_hbm.at[0], w_down.at[0], weight_sem.at[2]),
     ]
-    hidden_rows[...] = jnp.zeros_like(hidden_rows)
-
-    block_len = 256 if cache_len % 256 == 0 else 128
-    n_blocks = cache_len // block_len
-    triangle = (
-        iota((block_len, block_len), 0) > iota((block_len, block_len), 1)
-    ).astype(BF16)
-    flat = rows * heads
-    seq_col = lax.rem(iota((flat, 1), 0), rows)
-    head_col = iota((flat, 1), 0) // rows
-
-    token_load.wait()
-    rows_f32 = tokens[...].astype(F32)
-    gain_load.wait()
-    normed = (
-        rows_f32
-        * lax.rsqrt(jnp.mean(rows_f32 * rows_f32, axis=1, keepdims=True) + EPSILON)
-        * attn_gain[...]
-    ).astype(BF16)
-    query_load.wait()
     queries = dot(normed, w_query[...]).astype(BF16).astype(F32)
     for head in range(heads):
         first = head // group * HEAD_SIZE
@@ -222,8 +215,7 @@
     for head in range(heads):
         bias_col = jnp.where(head_col == head, head_bias[head], bias_col)
 
-    for copy in cache_loads[:2]:
-        copy.wait()
+    key_load.wait()
     key_rows = keys[...].reshape(rows * key_cols, cache_len)
     scores = dot(query_block, key_rows) * HEAD_SIZE ** (-0.5) + bias_col
     in_cache = iota((flat, cache_len), 1) < length_col
@@ -253,8 +245,7 @@
         carried = carried + jnp.sum(part, axis=1, keepdims=True)
     tail_sum = jnp.concatenate(tails, axis=1)
     breaks = jnp.where(in_cache, jnp.exp(log_take + tail_sum), 0.0).astype(BF16)
-    for copy in cache_loads[2:]:
-        copy.wait()
+    value_load.wait()
     value_rows = values[...].reshape(rows * key_cols, cache_len)
     crossed = lax.dot_general(
         breaks, value_rows, (((1,), (1,)), ((), ())), preferred_element_type=F32
@@ -355,36 +346,41 @@
     hidden_act = jnp.concatenate(acts, axis=1)
     if share == 2:
         pltpu.make_async_copy(w_down.at[1], w_down.at[1], recv_sem.at[4]).wait()
-    expert_rows = dot(hidden_act, w_down[...].reshape(hidden_act.shape[1], -1)).astype(BF16)
-    for source in range(half):
-        for peer_tp in range(n_tp):
-            part = slice(peer_tp * slice_width, (peer_tp + 1) * slice_width)
-            for pair in range(pairs):
-                first = source * ROW_TILE + 2 * pair
-                out_parts[peer_tp, source, pair] = expert_rows[first : first + 2, part]
     out_slot = returned.at[ep * chips + chip]
-
-    def far_owner(step):
-        return jnp.where(2 * ep >= 2 * first_ep + half, step, half - 1 - step)
-
-    def send_out(step):
-        source = far_owner(step)
-        for peer_tp in tp_order[:-1]:
-            copy_to(out_parts.at[peer_tp, source], out_slot, 2, first_ep + source, peer_tp)
-
-    def send_own(step):
-        source = far_owner(step)
-
-        @pl.when(first_ep + source != ep)
-        def _():
-            copy_to(out_parts.at[tp, source], out_slot, 2, first_ep + source, tp)
-
-        @pl.when(first_ep + source == ep)
-        def _():
-            pltpu.make_async_copy(out_parts.at[tp, source], out_slot, recv_sem.at[2]).start()
-
-    repeat(half, send_out)
-    repeat(half, send_own)
+    chip_width = share * slice_width
+    for order, peer_chip in enumerate(other_chips + [chip]):
+        cols = pl.ds(pl.multiple_of(peer_chip * chip_width, chip_width), chip_width)
+        down = w_down[:, :, cols].reshape(hidden_act.shape[1], chip_width)
+        expert_rows = dot(hidden_act, down).astype(BF16)
+        for source in range(half):
+            for member in range(share):
+                part = slice(member * slice_width, (member + 1) * slice_width)
+                for pair in range(pairs):
+                    first = source * ROW_TILE + 2 * pair
+                    out_parts[order, member, source, pair] = expert_rows[first : first + 2, part]
+
+        def send_out(step):
+            source = jnp.where(2 * ep >= 2 * first_ep + half, step, half - 1 - step)
+            owner = first_ep + source
+            if order < chips - 1:
+                for member in range(share):
+                    peer_tp = peer_chip * share + member
+                    copy_to(out_parts.at[order, member, source], out_slot, 2, owner, peer_tp)
+                return
+            if share == 2:
+                copy_to(out_parts.at[order, 1 - side, source], out_slot, 2, owner, partner)
+
+            @pl.when(owner != ep)
+            def _():
+                copy_to(out_parts.at[order, side, source], out_slot, 2, owner, tp)
+
+            @pl.when(owner == ep)
+            def _():
+                pltpu.make_async_copy(
+                    out_parts.at[order, side, source], out_slot, recv_sem.at[2]
+                ).start()
+
+        repeat(half, send_out)
     pltpu.make_async_copy(returned, returned, recv_sem.at[2]).wait()
 
     def expert_part(number):
@@ -492,11 +488,11 @@
         pltpu.VMEM((pairs, 2, slice_width), BF16),
         pltpu.VMEM((half, n_tp, pairs, 2, slice_width), BF16),
         pltpu.VMEM((half * ROW_TILE, width), F32),
-        pltpu.VMEM((n_tp, half, pairs, 2, slice_width), BF16),
+        pltpu.VMEM((n_tp // share, share, half, pairs, 2, slice_width), BF16),
         pltpu.VMEM((n_messages, pairs, 2, slice_width), BF16),
         pltpu.SemaphoreType.DMA((10,)),
-        pltpu.SemaphoreType.DMA((4,)),
-        pltpu.SemaphoreType.DMA((4,)),
+        pltpu.SemaphoreType.DMA((2,)),
+        pltpu.SemaphoreType.DMA((3,)),
         pltpu.SemaphoreType.DMA((5,)),
         pltpu.SemaphoreType.DMA((5,)),
     ]

time: 20.7 us -> 18.9 us (0.913)
  Pallas kernels: 19.9 us -> 18.1 us
    pallas_call x1, Pallas kernels: 19.3 us -> 17.5 us  [shards(): pl.pallas_call(functools.partial(layer_kernel, n_ep, n_tp, n_messages), o...]
where the time goes in v3:
time: 18.9 us; the launch traced here: 18.7 us
  Pallas kernels  18.1 us (96%)
  between operations  0.65 us (3%)
    pallas_call x1, Pallas kernels, shards(): pl.pallas_call(functools.partial(layer_kernel, n_ep, n_tp, n_messages), o...  17.5 us
    pallas_call x1, Pallas kernels, shards(): pl.pallas_call(place_results, out_shape=tuple((jax.ShapeDtypeStruct(r.sha...  0.63 us

profile of v3, /device:TPU:0, one launch (start us, length us, event | category | flops | bytes accessed | tf_op | source)
XLA Modules:
  0.0 18.7 jit_solution(10552037725559608468)
XLA Ops:
  0.6 17.5 %layer.1 = (bf16[10,256]{1,0:T(8,128)(2,1)S(1)}, bf16[10,128]{1,0:T(8,128)(2,1)S(1)}, bf16[10,128]{1,0:T(8,128)(2,1)S(1)}) custom-call(bf16[10,1024]{1,0:T(8,128)(2,1)} %tokens_hbm.1, f32[1,1024]{1,0:T(1,128)} %bitcast.4, bf16[1024,256]{1,0:T(8,128)(2,1)} %w_query_hbm.1, bf16[1024,128]{1,0:T(8,128)(2,1)} %w_key_hbm.1, bf16[1024,128]{1,0:T(8,128)(2,1)} %w_value_hbm.1, ...), custom_call_target="tpu_custom_call" | custom-call | tf_op jit(solution)/shard_map/layer/pallas_call | solution.py:499
  18.1 0.6 %place.1 = (bf16[10,256]{1,0:T(8,128)(2,1)}, bf16[10,128]{1,0:T(8,128)(2,1)}, bf16[10,128]{1,0:T(8,128)(2,1)}) custom-call(bf16[10,256]{1,0:T(8,128)(2,1)S(1)} %get-tuple-element.6.refs_0_, bf16[10,128]{1,0:T(8,128)(2,1)S(1)} %get-tuple-element.7.refs_1_, bf16[10,128]{1,0:T(8,128)(2,1)S(1)} %get-tuple-element.8.refs_2_), custom_call_target="tpu_custom_call" | custom-call | tf_op jit(solution)/shard_map/place/pallas_call | solution.py:514

commit v4 on v3

--- a/solution.py
+++ b/solution.py
@@ -62,10 +62,14 @@
     w_in,
     w_down,
     spread,
-    head_part,
-    head_all,
+    heads_near,
+    heads_far,
+    head_rows,
+    near_hidden,
+    partial_acts,
     hidden_part,
-    hidden_all,
+    hidden_near,
+    hidden_far,
     hidden_rows,
     out_parts,
     returned,
@@ -174,6 +178,12 @@
         * attn_gain[...]
     ).astype(BF16)
     query_load.wait()
+    for number, source in enumerate((w_gate_hbm, w_up_hbm)):
+        pltpu.make_async_copy(source.at[0], w_in.at[0, number], weight_sem.at[1]).start()
+    weight_loads = [
+        pltpu.make_async_copy(w_in.at[0], w_in.at[0], weight_sem.at[1]),
+        load(w_down_hbm.at[0], w_down.at[0], weight_sem.at[2]),
+    ]
     own_loads = [
         load(w_key_hbm, w_key, small_sem.at[5]),
         load(w_value_hbm, w_value, small_sem.at[9]),
@@ -183,12 +193,6 @@
         load(ffn_gain_hbm, ffn_gain, small_sem.at[6]),
         load(route_ids_hbm, route_ids, small_sem.at[7]),
         load(route_weights_hbm, route_weights, small_sem.at[8]),
-    ]
-    for number, source in enumerate((w_gate_hbm, w_up_hbm)):
-        pltpu.make_async_copy(source.at[0], w_in.at[0, number], weight_sem.at[1]).start()
-    weight_loads = [
-        pltpu.make_async_copy(w_in.at[0], w_in.at[0], weight_sem.at[1]),
-        load(w_down_hbm.at[0], w_down.at[0], weight_sem.at[2]),
     ]
     queries = dot(normed, w_query[...]).astype(BF16).astype(F32)
     for head in range(heads):
@@ -254,27 +258,49 @@
     for row in range(rows):
         own = jnp.where(seq_col == row, crossed[:, row * key_cols : (row + 1) * key_cols], own)
     spread[...] = own
-    heads_out = jnp.concatenate(
-        [
-            spread[
-                head * rows : (head + 1) * rows,
-                head // group * HEAD_SIZE : (head // group + 1) * HEAD_SIZE,
-            ]
-            for head in range(heads)
-        ],
-        axis=1,
-    ).astype(BF16)
+    key_lane = iota((rows, key_cols), 1) // HEAD_SIZE
+    tiles = []
+    for place in range(group):
+        tile = spread[place * rows : (place + 1) * rows, :]
+        for key_head in range(1, heads // group):
+            head = key_head * group + place
+            tile = jnp.where(key_lane == key_head, spread[head * rows : (head + 1) * rows, :], tile)
+        tiles.append(tile)
+    heads_out = jnp.concatenate(tiles, axis=1).astype(BF16)
 
     pl.semaphore_wait(barrier, n_ep + n_tp - 2)
-    head_part[...] = heads_out
-    own_cols = pl.ds(pl.multiple_of(tp * query_cols, query_cols), query_cols)
-    head_slot = head_all.at[:, own_cols]
-    for peer_tp in tp_order[:-1]:
-        copy_to(head_part, head_slot, 0, ep, peer_tp)
-    pltpu.make_async_copy(head_part, head_slot, recv_sem.at[0]).start()
+    def put_pairs(target, value):
+        for pair in range(pairs):
+            target[pair] = value[2 * pair : 2 * pair + 2]
+
+    def chip_heads(parts):
+        for member in range(share):
+            for pair in range(pairs):
+                head_rows[
+                    2 * pair : 2 * pair + 2, member * query_cols : (member + 1) * query_cols
+                ] = parts[member, pair].astype(F32)
+        return head_rows[...].astype(BF16)
+
+    def chip_projection(parts, peer_chip):
+        first = pl.multiple_of(peer_chip * share * query_cols, HEAD_SIZE)
+        out_rows = [
+            w_out[pl.ds(first + offset, HEAD_SIZE), :]
+            for start in range(0, share * query_cols, query_cols)
+            for place in range(group)
+            for offset in range(start + place * HEAD_SIZE, start + query_cols, group * HEAD_SIZE)
+        ]
+        return dot(chip_heads(parts), jnp.concatenate(out_rows, axis=0))
+
+    head_part = heads_near.at[side]
+    put_pairs(head_part, heads_out)
+    for step, peer_chip in enumerate(other_chips):
+        for member in range(share):
+            target = heads_far.at[chips - 2 - step, side]
+            copy_to(head_part, target, 5, ep, peer_chip * share + member)
     partner = tp + 1 - 2 * side
-    for copy in weight_loads:
-        copy.wait()
+    if share == 2:
+        copy_to(head_part, head_part, 0, ep, partner)
+    weight_loads[0].wait()
     if share == 2:
         copy_to(w_in.at[0], w_in.at[1], 3, ep, partner)
     for copy in own_loads:
@@ -282,34 +308,44 @@
     new_keys_ref[...] = dot(normed, w_key[...]).astype(BF16)
     new_values_ref[...] = dot(normed, w_value[...]).astype(BF16)
     out_load.wait()
-    pltpu.make_async_copy(head_all, head_all, recv_sem.at[0]).wait()
-    attn_out = dot(head_all[...], w_out[...])
-
     slice_cols = pl.ds(pl.multiple_of(tp * slice_width, slice_width), slice_width)
-    own_hidden = tokens[:, slice_cols].astype(F32) + attn_out
-    rounded = own_hidden.astype(BF16)
-    for pair in range(pairs):
-        hidden_part[pair] = rounded[2 * pair : 2 * pair + 2]
-    hidden_slot = hidden_all.at[lax.rem(ep, half), tp]
-
-    def send_hidden(step):
-        for peer_chip in other_chips + [chip]:
-            copy_to(hidden_part, hidden_slot, 1, far_ep(step), peer_chip * share + keeper)
-
-    repeat(n_ep - 1, send_hidden)
-    for peer_chip in other_chips:
-        copy_to(hidden_part, hidden_slot, 1, ep, peer_chip * share + keeper)
+    own_hidden = tokens[:, slice_cols].astype(F32)
+    if share == 2:
+        pltpu.make_async_copy(head_part, head_part, recv_sem.at[0]).wait()
+    near_hidden[...] = own_hidden + chip_projection(heads_near, chip)
+    pltpu.make_async_copy(heads_far, heads_far, recv_sem.at[5]).wait()
+    own_hidden = near_hidden[...]
+    for step, peer_chip in enumerate(other_chips):
+        own_hidden = own_hidden + chip_projection(heads_far.at[step], peer_chip)
+
+    put_pairs(hidden_part, own_hidden.astype(BF16))
+    row_slot = lax.rem(ep, half)
+    near_slot = hidden_near.at[row_slot, side]
+
+    def send_hidden(peer_ep):
+        for step, peer_chip in enumerate(other_chips):
+            target = hidden_far.at[chips - 2 - step, row_slot, side]
+            copy_to(hidden_part, target, 6, peer_ep, peer_chip * share + keeper)
+
+    def send_hidden_far(step):
+        send_hidden(far_ep(step))
+        copy_to(hidden_part, near_slot, 1, far_ep(step), chip * share + keeper)
+
+    repeat(n_ep - 1, send_hidden_far)
+    send_hidden(ep)
 
     @pl.when(mine)
     def _():
-        pltpu.make_async_copy(hidden_part, hidden_slot, recv_sem.at[1]).start()
+        pltpu.make_async_copy(hidden_part, near_slot, recv_sem.at[1]).start()
 
     if share == 2:
 
         @pl.when(jnp.logical_not(mine))
         def _():
-            copy_to(hidden_part, hidden_slot, 1, ep, partner)
-
+            copy_to(hidden_part, near_slot, 1, ep, partner)
+
+    weight_loads[1].wait()
+    if share == 2:
         copy_to(w_down.at[0], w_down.at[1], 4, ep, partner)
     for copy in route_loads:
         copy.wait()
@@ -326,28 +362,45 @@
         )
     if share == 2:
         pltpu.make_async_copy(w_in.at[1], w_in.at[1], recv_sem.at[3]).wait()
-    pltpu.make_async_copy(hidden_all, hidden_all, recv_sem.at[1]).wait()
-    for source in range(half):
-        for peer_tp in range(n_tp):
-            part = slice(peer_tp * slice_width, (peer_tp + 1) * slice_width)
-            for pair in range(pairs):
-                first = source * ROW_TILE + 2 * pair
-                hidden_rows[first : first + 2, part] = hidden_all[
-                    source, peer_tp, pair
-                ].astype(F32)
-    hidden = hidden_rows[...]
-    scaled = (hidden * ffn_gain[...]).astype(BF16)
-    row_scale = lax.rsqrt(jnp.mean(hidden * hidden, axis=1, keepdims=True) + EPSILON)
+    chip_width = share * slice_width
+
+    def chip_rows(parts, target, peer_chip):
+        for source in range(half):
+            for member in range(share):
+                part = slice(member * slice_width, (member + 1) * slice_width)
+                for pair in range(pairs):
+                    first = source * ROW_TILE + 2 * pair
+                    target[first : first + 2, part] = parts[source, member, pair].astype(F32)
+        hidden = target[...]
+        cols = pl.ds(pl.multiple_of(peer_chip * chip_width, chip_width), chip_width)
+        scaled = (hidden * ffn_gain[:, cols]).astype(BF16)
+        terms = [
+            dot(scaled, w_in[member, kind, cols, :])
+            for member in range(share)
+            for kind in range(2)
+        ]
+        return jnp.sum(hidden * hidden, axis=1, keepdims=True), terms
+
+    pltpu.make_async_copy(hidden_near, hidden_near, recv_sem.at[1]).wait()
+    squares, near_terms = chip_rows(hidden_near, hidden_rows.at[0], chip)
+    for number, term in enumerate(near_terms):
+        partial_acts[number] = term
+    pltpu.make_async_copy(hidden_far, hidden_far, recv_sem.at[6]).wait()
+    terms = [partial_acts[number] for number in range(2 * share)]
+    for step, peer_chip in enumerate(other_chips):
+        more, others = chip_rows(hidden_far.at[step], hidden_rows.at[step + 1], peer_chip)
+        squares = squares + more
+        terms = [term + other for term, other in zip(terms, others)]
+    row_scale = lax.rsqrt(squares * (1.0 / (n_tp * slice_width)) + EPSILON)
     acts = []
     for member in range(share):
-        gate_act = dot(scaled, w_in[member, 0]) * row_scale
-        up_act = dot(scaled, w_in[member, 1]) * row_scale
+        gate_act = terms[2 * member] * row_scale
+        up_act = terms[2 * member + 1] * row_scale
         acts.append((gate_act / (1.0 + jnp.exp(-gate_act)) * up_act).astype(BF16))
     hidden_act = jnp.concatenate(acts, axis=1)
     if share == 2:
         pltpu.make_async_copy(w_down.at[1], w_down.at[1], recv_sem.at[4]).wait()
     out_slot = returned.at[ep * chips + chip]
-    chip_width = share * slice_width
     for order, peer_chip in enumerate(other_chips + [chip]):
         cols = pl.ds(pl.multiple_of(peer_chip * chip_width, chip_width), chip_width)
         down = w_down[:, :, cols].reshape(hidden_act.shape[1], chip_width)
@@ -399,18 +452,22 @@
         mixed = mixed + scale * total.astype(BF16).astype(F32)
     mixed_ref[...] = mixed.astype(BF16)
 
-    sent = head_all.at[:, pl.ds(0, (n_tp - 1) * query_cols)]
-    pltpu.make_async_copy(sent, sent, send_sem.at[0]).wait()
-    for number in (1, 2):
+    pltpu.make_async_copy(heads_far, heads_far, send_sem.at[5]).wait()
+    if share == 2:
+        pltpu.make_async_copy(head_part, head_part, send_sem.at[0]).wait()
+    sent_far = returned.at[pl.ds(0, n_ep * (chips - 1))]
+    pltpu.make_async_copy(sent_far, sent_far, send_sem.at[6]).wait()
+    for number, most in ((1, n_ep), (2, n_messages)):
 
         @pl.when(mine)
         def _():
-            sent = returned.at[pl.ds(0, n_messages - 1)]
+            sent = returned.at[pl.ds(0, most - 1)]
             pltpu.make_async_copy(sent, sent, send_sem.at[number]).wait()
 
         @pl.when(jnp.logical_not(mine))
         def _():
-            pltpu.make_async_copy(returned, returned, send_sem.at[number]).wait()
+            sent = returned.at[pl.ds(0, most)]
+            pltpu.make_async_copy(sent, sent, send_sem.at[number]).wait()
 
     if share == 2:
         pltpu.make_async_copy(w_in.at[1], w_in.at[1], send_sem.at[3]).wait()
@@ -476,25 +533,29 @@
         for number, operand in enumerate(operands[:13])
     ]
     share = 2 if n_ep % 2 == 0 and n_tp % 2 == 0 else 1
-    half, pairs = n_ep // share, rows // 2
+    half, chips, pairs = n_ep // share, n_tp // share, rows // 2
     n_messages = half * n_tp
     hidden_units = w_gate.shape[2]
     scratch = buffers + [
         pltpu.VMEM((share, 2, width, hidden_units), BF16),
         pltpu.VMEM((share, hidden_units, width), BF16),
         pltpu.VMEM((rows * (query_cols // HEAD_SIZE), key_cols), F32),
-        pltpu.VMEM((rows, query_cols), BF16),
-        pltpu.VMEM((rows, query_cols * n_tp), BF16),
+        pltpu.VMEM((share, pairs, 2, query_cols), BF16),
+        pltpu.VMEM((chips - 1, share, pairs, 2, query_cols), BF16),
+        pltpu.VMEM((rows, share * query_cols), F32),
+        pltpu.VMEM((rows, slice_width), F32),
+        pltpu.VMEM((2 * share, half * ROW_TILE, hidden_units), F32),
         pltpu.VMEM((pairs, 2, slice_width), BF16),
-        pltpu.VMEM((half, n_tp, pairs, 2, slice_width), BF16),
-        pltpu.VMEM((half * ROW_TILE, width), F32),
-        pltpu.VMEM((n_tp // share, share, half, pairs, 2, slice_width), BF16),
+        pltpu.VMEM((half, share, pairs, 2, slice_width), BF16),
+        pltpu.VMEM((chips - 1, half, share, pairs, 2, slice_width), BF16),
+        pltpu.VMEM((chips, half * ROW_TILE, share * slice_width), F32),
+        pltpu.VMEM((chips, share, half, pairs, 2, slice_width), BF16),
         pltpu.VMEM((n_messages, pairs, 2, slice_width), BF16),
         pltpu.SemaphoreType.DMA((10,)),
         pltpu.SemaphoreType.DMA((2,)),
         pltpu.SemaphoreType.DMA((3,)),
-        pltpu.SemaphoreType.DMA((5,)),
-        pltpu.SemaphoreType.DMA((5,)),
+        pltpu.SemaphoreType.DMA((7,)),
+        pltpu.SemaphoreType.DMA((7,)),
     ]
     results = pl.pallas_call(
         functools.partial(layer_kernel, n_ep, n_tp, n_messages),

time: 18.9 us -> 18.5 us (0.979)
  Pallas kernels: 18.1 us -> 17.8 us
    pallas_call x1, Pallas kernels: 17.5 us -> 17.1 us  [shards(): pl.pallas_call(functools.partial(layer_kernel, n_ep, n_tp, n_messages), o...]
where the time goes in v4:
time: 18.5 us; the launch traced here: 18.4 us
  Pallas kernels  17.8 us (96%)
  between operations  0.65 us (4%)
    pallas_call x1, Pallas kernels, shards(): pl.pallas_call(functools.partial(layer_kernel, n_ep, n_tp, n_messages), o...  17.1 us
    pallas_call x1, Pallas kernels, shards(): pl.pallas_call(place_results, out_shape=tuple((jax.ShapeDtypeStruct(r.sha...  0.63 us

profile of v4, /device:TPU:0, one launch (start us, length us, event | category | flops | bytes accessed | tf_op | source)
XLA Modules:
  0.0 18.4 jit_solution(8664571085385800414)
XLA Ops:
  0.6 17.1 %layer.1 = (bf16[10,256]{1,0:T(8,128)(2,1)S(1)}, bf16[10,128]{1,0:T(8,128)(2,1)S(1)}, bf16[10,128]{1,0:T(8,128)(2,1)S(1)}) custom-call(bf16[10,1024]{1,0:T(8,128)(2,1)} %tokens_hbm.1, f32[1,1024]{1,0:T(1,128)} %bitcast.4, bf16[1024,256]{1,0:T(8,128)(2,1)} %w_query_hbm.1, bf16[1024,128]{1,0:T(8,128)(2,1)} %w_key_hbm.1, bf16[1024,128]{1,0:T(8,128)(2,1)} %w_value_hbm.1, ...), custom_call_target="tpu_custom_call" | custom-call | tf_op jit(solution)/shard_map/layer/pallas_call | solution.py:560
  17.8 0.6 %place.1 = (bf16[10,256]{1,0:T(8,128)(2,1)}, bf16[10,128]{1,0:T(8,128)(2,1)}, bf16[10,128]{1,0:T(8,128)(2,1)}) custom-call(bf16[10,256]{1,0:T(8,128)(2,1)S(1)} %get-tuple-element.6.refs_0_, bf16[10,128]{1,0:T(8,128)(2,1)S(1)} %get-tuple-element.7.refs_1_, bf16[10,128]{1,0:T(8,128)(2,1)S(1)} %get-tuple-element.8.refs_2_), custom_call_target="tpu_custom_call" | custom-call | tf_op jit(solution)/shard_map/place/pallas_call | solution.py:575
